TPU v7x, 32 devices: a whole 2x2x4 slice. The times are simulated.
32 devices in a mesh: kv: 8 (over z, x), tp: 4 (over y, core).
Axes of the slice: x: 2, y: 2, z: 4, core: 2. Of those that a mesh axis runs over, the one named last changes fastest.
Arguments:
- hidden: bfloat16 [128, 4, 2048], P(None, None, 'kv'), may hold values from -18 to 18
- norm_gain: float32 [2048], replicated, may hold values from 0.1 to 1.9
- w_query: bfloat16 [2048, 1024], P(None, 'tp'), may hold values from -0.125 to 0.125
- w_forget: bfloat16 [2048, 1024], P(None, 'tp'), may hold values from -0.125 to 0.125
- w_input: bfloat16 [2048, 1024], P(None, 'tp'), may hold values from -0.125 to 0.125
- w_outgate: bfloat16 [2048, 1024], P(None, 'tp'), may hold values from -0.125 to 0.125
- w_out: bfloat16 [1024, 2048], replicated, may hold values from -0.1875 to 0.1875
- floor: float32 [1024], P('tp'), may hold values from 0 to 0.95
- head_gain: float32 [128], replicated, may hold values from 0.1 to 1.9
- base_state: float32 [128, 8, 128, 128], P('kv', 'tp'), may hold values from -4 to 4
- prev_forget: bfloat16 [128, 4, 1024], P('kv', None, 'tp'), may hold values from -6 to 6
- prev_input: bfloat16 [128, 4, 1024], P('kv', None, 'tp'), may hold values from -6 to 6
- accepted: int32 [128], P('kv'), may hold values from 0 to 4
Outputs:
- mixed: bfloat16 [128, 4, 2048], P(None, None, 'kv')
- taken_state: float32 [128, 8, 128, 128], P('kv', 'tp')
All inputs are finite; a program needn't handle non-finite values.
Results may differ from a plain program's by a relative error of at most 0.014.
Values may be sent and summed in bfloat16 or wider, within the bound.
A program may use at most 64 MiB of HBM per device.

v0:
```python
import jax
import jax.numpy as jnp
from jax import lax
from jax.sharding import PartitionSpec as P

D = 2048
HEAD_DIM = 128
PROPS = 4


def shards(
    hidden,
    norm_gain,
    w_query,
    w_forget,
    w_input,
    w_outgate,
    w_out,
    floor,
    head_gain,
    base_state,
    prev_forget,
    prev_input,
    accepted,
):
    arrived = lax.all_to_all(hidden, "kv", split_axis=0, concat_axis=2, tiled=True)
    whole_vals = arrived.astype(jnp.float32)
    row_sums = jnp.sum(whole_vals * whole_vals, axis=2)
    normed = (whole_vals * lax.rsqrt(row_sums / D + 1e-06)[..., None] * norm_gain).astype(
        jnp.bfloat16
    )
    query_pre = jnp.dot(normed, w_query, preferred_element_type=jnp.float32).astype(jnp.bfloat16)
    forget_pre = jnp.dot(normed, w_forget, preferred_element_type=jnp.float32).astype(jnp.bfloat16)
    input_pre = jnp.dot(normed, w_input, preferred_element_type=jnp.float32).astype(jnp.bfloat16)
    gate_pre = jnp.dot(normed, w_outgate, preferred_element_type=jnp.float32).astype(jnp.bfloat16)
    seq_local = normed.shape[0]
    head_local = w_query.shape[1] // HEAD_DIM
    shape = (seq_local, PROPS, head_local, HEAD_DIM)
    query = jax.nn.silu(query_pre.astype(jnp.float32)).reshape(shape)
    forget = (floor + (1.0 - floor) * jax.nn.sigmoid(forget_pre.astype(jnp.float32))).reshape(shape)
    value = input_pre.astype(jnp.float32).reshape(shape)
    prev_f = (floor + (1.0 - floor) * jax.nn.sigmoid(prev_forget.astype(jnp.float32))).reshape(
        shape
    )
    prev_v = prev_input.astype(jnp.float32).reshape(shape)
    state = base_state
    for step in range(PROPS):
        live = (step < accepted)[:, None, None, None]
        moved = (
            prev_f[:, step][..., None] * state
            + (1.0 - prev_f[:, step])[..., None] * prev_v[:, step][:, :, None, :]
        )
        state = jnp.where(live, moved, state)
    taken_state = state
    outputs = []
    for step in range(PROPS):
        state = (
            forget[:, step][..., None] * state
            + (1.0 - forget[:, step])[..., None] * value[:, step][:, :, None, :]
        )
        outputs.append(
            jnp.einsum("bhk,bhkv->bhv", query[:, step], state, precision=lax.Precision.HIGHEST)
        )
    result = jnp.stack(outputs, axis=1)
    scaled = (
        result * lax.rsqrt(jnp.mean(result * result, axis=-1, keepdims=True) + 1e-05) * head_gain
    )
    gated = scaled * jax.nn.silu(gate_pre.astype(jnp.float32)).reshape(shape)
    mixed_heads = gated.reshape(seq_local, PROPS, head_local * HEAD_DIM).astype(jnp.bfloat16)
    own_rows = mixed_heads.shape[2]
    w_rows = lax.dynamic_slice_in_dim(w_out, lax.axis_index("tp") * own_rows, own_rows, 0)
    partial_value = jnp.dot(mixed_heads, w_rows, preferred_element_type=jnp.float32)
    finished = lax.psum(partial_value, "tp").astype(jnp.bfloat16)
    mixed = lax.all_to_all(finished, "kv", split_axis=2, concat_axis=0, tiled=True)
    return (mixed, taken_state)


def solution(mesh):
    placed = (
        P(None, None, "kv"),
        P(),
        P(None, "tp"),
        P(None, "tp"),
        P(None, "tp"),
        P(None, "tp"),
        P(),
        P("tp"),
        P(),
        P("kv", "tp", None, None),
        P("kv", None, "tp"),
        P("kv", None, "tp"),
        P("kv"),
    )
    return jax.shard_map(
        shards,
        mesh=mesh,
        in_specs=placed,
        out_specs=(P(None, None, "kv"), P("kv", "tp", None, None)),
        check_vma=False,
    )
```

profile of v0, /device:TPU:0, one launch (start us, length us, event | category | flops | bytes accessed | tf_op | source)
XLA Modules:
  0.0 96.0 jit_solution(18002514994027775703)
XLA Ops:
  0.6 0.0 copy-start
  0.6 7.4 %all-to-all-start = ((bf16[128,4,256]{2,1,0:T(4,128)(2,1)}), bf16[128,4,256]{2,1,0:T(4,128)(2,1)S(1)}, u32[]{:S(2)}, u32[]{:S(2)}) async-start(bf16[128,4,256]{2,1,0:T(4,128)(2,1)} %param.13), calls=%async_computation | async-start | bytes 524288 | tf_op jit(solution)/shard_map/all_to_all | solution.py:26
  8.1 0.7 broadcast_subtract_fusion.8
  8.8 0.6 copy-done.3
  9.3 0.8 multiply_add_fusion.9
  10.2 1.2 %broadcast_bitcast_fusion = f32[256]{0:T(256)} fusion(f32[128]{0:T(128)} %param.21), kind=kLoop, calls=%fused_computation.82 | loop fusion | bytes 1536 | tf_op jit(solution)/shard_map/mul | solution.py:66
  11.5 1.3 %broadcast_compare_fusion.3 = (pred[16]{0:T(512)(128)(4,1)}, pred[16]{0:T(512)(128)(4,1)}, pred[16]{0:T(512)(128)(4,1)}, pred[16]{0:T(512)(128)(4,1)}) fusion(s32[16]{0:T(128)} %param.25), kind=kLoop, calls=%fused_computation.88 | loop fusion | flops 64 | bytes 128 | tf_op jit(solution)/shard_map/gt | solution.py:48
  12.7 0.8 reshape.130
  13.5 0.6 slice_bitcast_fusion.10
  14.1 7.1 %add_select_fusion = f32[16,2,128,128]{3,2,1,0:T(8,128)S(1)} fusion(f32[16,2,128,128]{3,2,1,0:T(8,128)} %param.22, f32[16,2,128]{2,1,0:T(2,128)} %get-tuple-element.29, f32[16,2,128]{2,1,0:T(2,128)S(1)} %get-tuple-element.25, f32[16,2,128]{2,1,0:T(2,128)} %get-tuple-element.27, f32[16,2,128]{2,1,0:T(2,128)S(1)} %get-tuple-element.24, ...), kind=kLoop, calls=%fused_computation.7 | loop fusion | flops 8388608 | bytes 4390976 | tf_op jit(solution)/shard_map/jit(_where)/select_n | solution.py:53
  21.3 0.0 copy-start.1
  21.3 0.0 copy-start.5
  21.3 0.0 copy-start.2
  21.3 0.0 copy-start.4
  21.3 0.0 all-to-all-done
  21.3 0.2 multiply_reduce_fusion
  21.6 0.1 copy.55
  21.7 0.1 convert_element_type.70
  21.7 1.1 %copy.38 = f32[16,4,8,256]{3,2,0,1:T(8,128)} copy(f32[16,4,8,256]{3,1,0,2:T(4,128)S(1)} %bitcast.141) | data formatting | bytes 1048576 | tf_op jit(solution)/shard_map/convert_element_type | solution.py:27
  22.8 1.9 %reshape.128 = f32[16,4,2048]{2,0,1:T(8,128)} reshape(f32[16,4,8,256]{3,2,0,1:T(8,128)} %copy.38) | data formatting | bytes 1048576 | tf_op jit(solution)/shard_map/convert_element_type | solution.py:27
  24.8 0.0 copy-done.5
  24.8 1.2 %multiply_convert_fusion = bf16[16,4,2048]{2,0,1:T(8,128)(2,1)S(1)} fusion(f32[16,4,2048]{2,0,1:T(8,128)} %reshape.128, f32[2048]{0:T(1024)S(1)} %copy-done.5, f32[16,4]{0,1:T(4,128)S(1)} %add_rsqrt_fusion.1), kind=kLoop, calls=%fused_computation.43 | loop fusion | flops 393216 | bytes 794880 | tf_op jit(solution)/shard_map/convert_element_type | solution.py:29
  25.9 0.0 copy-done.2
  25.9 0.0 copy-done.4
  25.9 1.5 %fusion.14 = f32[16,4,256]{2,0,1:T(8,128)S(1)} fusion(bf16[16,4,2048]{2,0,1:T(8,128)(2,1)S(1)} %multiply_convert_fusion, bf16[2048,256]{1,0:T(8,128)(2,1)} %param.16, f32[256]{0:T(256)S(1)} %copy-done.4, f32[256]{0:T(256)S(1)} %copy-done.2), kind=kOutput, calls=%fused_computation.21 | convolution fusion | flops 67223552 | bytes 1378304 | tf_op jit(solution)/shard_map/dot_general | solution.py:33
  27.5 1.5 %fusion.7 = f32[16,4,256]{2,0,1:T(8,128)S(1)} fusion(bf16[16,4,2048]{2,0,1:T(8,128)(2,1)S(1)} %multiply_convert_fusion, bf16[2048,256]{1,0:T(8,128)(2,1)} %param.17), kind=kOutput, calls=%fused_computation.13 | convolution fusion | flops 67141632 | bytes 1376256 | tf_op jit(solution)/shard_map/dot_general | solution.py:34
  29.1 0.7 reshape.132
  29.7 2.2 %divide_multiply_fusion = f32[16,4,256]{2,0,1:T(8,128)} fusion(bf16[16,4,2048]{2,0,1:T(8,128)(2,1)S(1)} %multiply_convert_fusion, bf16[2048,256]{1,0:T(8,128)(2,1)} %param.15), kind=kOutput, calls=%fused_computation.53 | convolution fusion | flops 67207168 | bytes 1376256 | tf_op jit(solution)/shard_map/dot_general | solution.py:32
  31.9 0.9 reshape.121
  32.8 0.8 slice_bitcast_fusion.6
  33.6 2.8 %fusion.4 = f32[16,2,1,128]{3,2,1,0:T(1,128)S(1)} fusion(f32[16,2,128,1]{2,3,1,0:T(1,128)S(1)} %bitcast.146, f32[16,2,128,128]{3,2,1,0:T(8,128)S(1)} %add_select_fusion, f32[16,2,128]{2,1,0:T(2,128)S(1)} %get-tuple-element.14, f32[16,2,128]{2,1,0:T(2,128)S(1)} %get-tuple-element.10, f32[16,2,128]{2,1,0:T(2,128)S(1)} %get-tuple-element.37), kind=kOutput, calls=%fused_computation.8 | convolution fusion | flops 7864320 | bytes 2179072 | tf_op jit(solution)/shard_map/bhk,bhkv->bhv/dot_general | solution.py:62
  36.4 4.3 %fusion.35 = f32[16,2,1,128]{3,2,1,0:T(1,128)S(1)} fusion(f32[16,2,128,1]{2,3,1,0:T(1,128)S(1)} %bitcast.155, f32[16,2,128,128]{3,2,1,0:T(8,128)S(1)} %add_select_fusion, f32[16,2,128]{2,1,0:T(2,128)S(1)} %get-tuple-element.17, f32[16,2,128]{2,1,0:T(2,128)S(1)} %get-tuple-element.13, f32[16,2,128]{2,1,0:T(2,128)S(1)} %get-tuple-element.34, ...), kind=kOutput, calls=%fused_computation.45 | convolution fusion | flops 9437184 | bytes 2228224 | tf_op jit(solution)/shard_map/bhk,bhkv->bhv/dot_general | solution.py:62
  40.7 6.1 %fusion.5 = f32[16,2,1,128]{3,2,1,0:T(1,128)S(1)} fusion(f32[16,2,128,1]{2,3,1,0:T(1,128)S(1)} %bitcast.154, f32[16,2,128]{2,1,0:T(2,128)S(1)} %get-tuple-element.16, f32[16,2,128]{2,1,0:T(2,128)S(1)} %get-tuple-element.12, f32[16,2,128]{2,1,0:T(2,128)S(1)} %get-tuple-element.35, f32[16,2,128,128]{3,2,1,0:T(8,128)S(1)} %add_select_fusion, ...), kind=kOutput, calls=%fused_computation.9 | convolution fusion | flops 11010048 | bytes 2277376 | tf_op jit(solution)/shard_map/bhk,bhkv->bhv/dot_general | solution.py:62
  46.8 0.0 copy-done.1
  46.8 0.0 copy-start.6
  46.8 7.2 %fusion = f32[16,2,1,128]{3,2,1,0:T(1,128)S(1)} fusion(f32[16,2,128,1]{2,3,1,0:T(1,128)S(1)} %bitcast.153, f32[16,2,128]{2,1,0:T(2,128)S(1)} %get-tuple-element.15, f32[16,2,128]{2,1,0:T(2,128)S(1)} %get-tuple-element.11, f32[16,2,128]{2,1,0:T(2,128)S(1)} %get-tuple-element.36, f32[16,2,128]{2,1,0:T(2,128)S(1)} %get-tuple-element.16, ...), kind=kOutput, calls=%fused_computation | convolution fusion | flops 12582912 | bytes 2326528 | tf_op jit(solution)/shard_map/bhk,bhkv->bhv/dot_general | solution.py:62
  54.1 0.1 fusion.39
  54.2 0.1 mul.343
  54.4 0.1 mul.344
  54.4 0.0 copy-done
  54.4 0.0 copy-done.6
  54.4 2.0 %fusion.16 = f32[16,4,2048]{2,0,1:T(8,128)S(1)} fusion(bf16[1024,2048]{1,0:T(8,128)(2,1)} %param.19, s32[]{:T(128)S(6)} %select_n.20, f32[16,4,256]{2,0,1:T(8,128)S(1)} %mul.344, f32[16,1,256]{2,0,1:T(8,128)S(1)} %stack.28, f32[16,1,256]{2,0,1:T(8,128)S(1)} %stack.27, f32[16,1,256]{2,0,1:T(8,128)S(1)} %stack.26, f32[16,1,256]{2,0,1:T(8,128)S(1)} %stack.25, ...), kind=kOutput, calls=%fused_computation.24 | convolution fusion | flops 134430720 | bytes 3015684 | tf_op jit(solution)/shard_map/dot_general | solution.py:72
  56.5 16.6 %all-reduce.1 = bf16[16,4,2048]{2,0,1:T(8,128)(2,1)S(1)} all-reduce(f32[16,4,2048]{2,0,1:T(8,128)S(1)} %fusion.16), channel_id=1, replica_groups=mesh['kv'=8,'tp'=4] {'tp'}, use_global_device_ids=true, to_apply=%region_3.4 | all-reduce | flops 131072 | bytes 786432 | tf_op jit(solution)/shard_map/psum | solution.py:73
  73.1 1.4 %copy.45 = bf16[16,4,2048]{0,1,2:T(4,128)(2,1)S(1)} copy(bf16[16,4,2048]{2,0,1:T(8,128)(2,1)S(1)} %all-reduce.1) | data formatting | bytes 524288 | tf_op jit(solution)/shard_map/convert_element_type | solution.py:73
  74.5 2.2 %reshape.148 = bf16[8,2,8192]{2,1,0:T(2,128)(2,1)S(1)} reshape(bf16[2048,4,16]{2,1,0:T(4,128)(2,1)S(1)} %bitcast.139) | data formatting | bytes 524288
  76.7 14.9 %all_to_all.27 = bf16[8,2,8192]{2,1,0:T(2,128)(2,1)} all-to-all(bf16[8,2,8192]{2,1,0:T(2,128)(2,1)S(1)} %reshape.148), channel_id=1, replica_groups=mesh['kv'=8,'tp'=4] {'kv'}, dimensions={0} | all-to-all | bytes 524288 | tf_op jit(solution)/shard_map/all_to_all | solution.py:74
  91.5 2.4 %reshape.149 = bf16[2048,4,16]{2,1,0:T(4,128)(2,1)S(1)} reshape(bf16[8,2,8192]{2,1,0:T(2,128)(2,1)} %all_to_all.27) | data formatting | bytes 524288
  94.0 2.0 %copy.46 = bf16[8,16,4,256]{3,2,1,0:T(4,128)(2,1)} copy(bf16[8,16,4,256]{1,2,3,0:T(4,128)(2,1)S(1)} %bitcast.140) | data formatting | bytes 524288 | tf_op jit(solution)/shard_map/all_to_all | solution.py:74
  (14 shorter events, 0.3 us)
Async XLA Ops:
  0.6 53.8 %copy-start = (bf16[2048,256]{1,0:T(8,128)(2,1)S(1)}, bf16[2048,256]{1,0:T(8,128)(2,1)}, u32[]{:S(2)}) copy-start(bf16[2048,256]{1,0:T(8,128)(2,1)} %param.18) | copy-start | bytes 3145732
  0.6 20.7 %all-to-all-start = ((bf16[128,4,256]{2,1,0:T(4,128)(2,1)}), bf16[128,4,256]{2,1,0:T(4,128)(2,1)S(1)}, u32[]{:S(2)}, u32[]{:S(2)}) async-start(bf16[128,4,256]{2,1,0:T(4,128)(2,1)} %param.13), calls=%async_computation | async-start | bytes 524288 | tf_op jit(solution)/shard_map/all_to_all | solution.py:26
  8.8 0.6 copy-start.3
  21.3 25.5 %copy-start.1 = (f32[16,2,128,128]{3,2,1,0:T(8,128)}, f32[16,2,128,128]{3,2,1,0:T(8,128)S(1)}, u32[]{:S(2)}) copy-start(f32[16,2,128,128]{3,2,1,0:T(8,128)S(1)} %add_select_fusion) | copy-start | bytes 6291460
  21.3 3.5 %copy-start.5 = (f32[2048]{0:T(1024)S(1)}, f32[2048]{0:T(1024)}, u32[]{:S(2)}) copy-start(f32[2048]{0:T(1024)} %param.14) | copy-start | bytes 24580
  21.3 4.6 %copy-start.2 = (f32[256]{0:T(256)S(1)}, f32[256]{0:T(256)}, u32[]{:S(2)}) copy-start(f32[256]{0:T(256)} %param.20) | copy-start | bytes 3076
  21.3 4.6 %copy-start.4 = (f32[256]{0:T(256)S(1)}, f32[256]{0:T(256)}, u32[]{:S(2)}) copy-start(f32[256]{0:T(256)} %copy-done.3) | copy-start | bytes 3076
  46.8 7.7 %copy-start.6 = (f32[256]{0:T(256)S(1)}, f32[256]{0:T(256)}, u32[]{:S(2)}) copy-start(f32[256]{0:T(256)} %broadcast_bitcast_fusion) | copy-start | bytes 3076
where the time goes:
time: 96.9 us; the launch traced here: 96 us
  blocking collectives  31.5 us (33%)
  matrix products  27.6 us (28%)
  local copies, waits for them, and re-layouts  17 us (18%)
  other arithmetic  11.5 us (12%)
  starting transfers between devices  7.42 us (8%)
    dot_general x4, matrix products, shards(): jnp.einsum('bhk,bhkv->bhv', query[:, step], state, precision=lax.Precisio...  20.3 us
    psum x1, blocking collectives, shards(): finished = lax.psum(partial_value, 'tp').astype(jnp.bfloat16)  16.6 us
    all_to_all x1, blocking collectives, shards(): lax.all_to_all(finished, 'kv', split_axis=2, concat_axis=0, tiled=True)  14.9 us
    all_to_all x1, starting transfers between devices, shards(): lax.all_to_all(hidden, 'kv', split_axis=0, concat_axis=2, tiled=True)  7.42 us
    select_n x1, other arithmetic, shards(): state = jnp.where(live, moved, state)  7.13 us
    unnamed x17, local copies, waits for them, and re-layouts  5.27 us
    convert_element_type x2, local copies, waits for them, and re-layouts, shards(): whole_vals = arrived.astype(jnp.float32)  3.03 us
    dot_general x1, matrix products, shards(): jnp.dot(normed, w_query, preferred_element_type=jnp.float32)  2.17 us
  transfers between devices with their start and end apart: 1, of which 0 were waited for; matrix products, arithmetic and copies ran while one was open for 13% of the time, Pallas kernels for 0%

commit v1 on v0

--- a/solution.py
+++ b/solution.py
@@ -70,7 +70,12 @@
     own_rows = mixed_heads.shape[2]
     w_rows = lax.dynamic_slice_in_dim(w_out, lax.axis_index("tp") * own_rows, own_rows, 0)
     partial_value = jnp.dot(mixed_heads, w_rows, preferred_element_type=jnp.float32)
-    finished = lax.psum(partial_value, "tp").astype(jnp.bfloat16)
+
+    def _push_axis_part(slab_in):
+        even = jnp.sum(lax.all_gather(slab_in, "tp"), 0)
+        return even
+
+    finished = _push_axis_part(partial_value).astype(jnp.bfloat16)
     mixed = lax.all_to_all(finished, "kv", split_axis=2, concat_axis=0, tiled=True)
     return (mixed, taken_state)
 

time: 96.9 us -> 120 us (1.24)
  waiting for transfers between devices: 0.01 us -> 24.1 us
  blocking collectives: 31.5 us -> 14.7 us
  between operations: 0.93 us -> 14.3 us
  other arithmetic: 11.5 us -> 13.3 us
    all_gather x0 -> x1, waiting for transfers between devices: none -> 24.1 us  [_push_axis_part(): even = jnp.sum(lax.all_gather(slab_in, 'tp'), 0)]
    psum x1 -> x0, blocking collectives: 16.6 us -> none  [shards(): finished = lax.psum(partial_value, 'tp').astype(jnp.bfloat16)]
    reduce_sum x0 -> x1, other arithmetic: none -> 1.78 us  [_push_axis_part(): even = jnp.sum(lax.all_gather(slab_in, 'tp'), 0)]
    unnamed x17 -> x18, local copies, waits for them, and re-layouts: 5.27 us -> 6.17 us
  transfers between devices with their start and end apart: 1 -> 2, of which waited for: 0 -> 1; matrix products, arithmetic and copies ran while one was open for 13% -> 11% of each run, Pallas kernels for 0% -> 0%
where the time goes in v1:
time: 120 us; the launch traced here: 119 us
  matrix products  28.4 us (24%)
  waiting for transfers between devices  24.1 us (20%)
  local copies, waits for them, and re-layouts  17 us (14%)
  blocking collectives  14.7 us (12%)
  between operations  14.3 us (12%)
  other arithmetic  13.3 us (11%)
  starting transfers between devices  7.46 us (6%)
    all_gather x1, waiting for transfers between devices, _push_axis_part(): even = jnp.sum(lax.all_gather(slab_in, 'tp'), 0)  24.1 us
    dot_general x4, matrix products, shards(): jnp.einsum('bhk,bhkv->bhv', query[:, step], state, precision=lax.Precisio...  20.3 us
    all_to_all x1, blocking collectives, shards(): lax.all_to_all(finished, 'kv', split_axis=2, concat_axis=0, tiled=True)  14.7 us
    all_to_all x1, starting transfers between devices, shards(): lax.all_to_all(hidden, 'kv', split_axis=0, concat_axis=2, tiled=True)  7.42 us
    select_n x1, other arithmetic, shards(): state = jnp.where(live, moved, state)  7.13 us
    unnamed x18, local copies, waits for them, and re-layouts  6.17 us
    convert_element_type x2, local copies, waits for them, and re-layouts, shards(): whole_vals = arrived.astype(jnp.float32)  3.01 us
    dot_general x1, matrix products, shards(): jnp.dot(mixed_heads, w_rows, preferred_element_type=jnp.float32)  2.85 us
  transfers between devices with their start and end apart: 2, of which 1 were waited for; matrix products, arithmetic and copies ran while one was open for 11% of the time, Pallas kernels for 0%

profile of v1, /device:TPU:0, one launch (start us, length us, event | category | flops | bytes accessed | tf_op | source)
XLA Modules:
  0.0 119.4 jit_solution(5883144368100798663)
XLA Ops:
  7.2 0.0 copy-start
  7.2 7.4 %all-to-all-start = ((bf16[128,4,256]{2,1,0:T(4,128)(2,1)}), bf16[128,4,256]{2,1,0:T(4,128)(2,1)S(1)}, u32[]{:S(2)}, u32[]{:S(2)}) async-start(bf16[128,4,256]{2,1,0:T(4,128)(2,1)} %param.13), calls=%async_computation | async-start | bytes 524288 | tf_op jit(solution)/shard_map/all_to_all | solution.py:26
  14.6 0.0 all-gather.3.cloned.1.call-start
  14.7 0.7 broadcast_subtract_fusion.8
  15.3 0.6 copy-done.3
  15.9 0.8 multiply_add_fusion.9
  16.8 1.2 %broadcast_bitcast_fusion = f32[256]{0:T(256)} fusion(f32[128]{0:T(128)} %param.21), kind=kLoop, calls=%fused_computation.82 | loop fusion | bytes 1536 | tf_op jit(solution)/shard_map/mul | solution.py:66
  18.0 1.2 %broadcast_compare_fusion.3 = (pred[16]{0:T(512)(128)(4,1)}, pred[16]{0:T(512)(128)(4,1)}, pred[16]{0:T(512)(128)(4,1)}, pred[16]{0:T(512)(128)(4,1)}) fusion(s32[16]{0:T(128)} %param.25), kind=kLoop, calls=%fused_computation.88 | loop fusion | flops 64 | bytes 128 | tf_op jit(solution)/shard_map/gt | solution.py:48
  19.3 0.8 reshape.130
  20.1 0.6 slice_bitcast_fusion.10
  20.7 7.1 %add_select_fusion = f32[16,2,128,128]{3,2,1,0:T(8,128)S(1)} fusion(f32[16,2,128,128]{3,2,1,0:T(8,128)} %param.22, f32[16,2,128]{2,1,0:T(2,128)} %get-tuple-element.39, f32[16,2,128]{2,1,0:T(2,128)S(1)} %get-tuple-element.35, f32[16,2,128]{2,1,0:T(2,128)} %get-tuple-element.37, f32[16,2,128]{2,1,0:T(2,128)S(1)} %get-tuple-element.34, ...), kind=kLoop, calls=%fused_computation.7 | loop fusion | flops 8388608 | bytes 4390976 | tf_op jit(solution)/shard_map/jit(_where)/select_n | solution.py:53
  27.8 0.0 copy-start.1
  27.8 0.0 copy-start.5
  27.9 0.0 copy-start.2
  27.9 0.0 all-to-all-done
  27.9 0.2 multiply_reduce_fusion
  28.1 0.1 copy.85
  28.2 0.1 convert_element_type.70
  28.3 1.1 copy.64
  29.4 1.9 %reshape.128 = f32[16,4,2048]{2,0,1:T(8,128)} reshape(f32[16,4,8,256]{3,2,0,1:T(8,128)} %copy.64) | data formatting | bytes 1048576 | tf_op jit(solution)/shard_map/convert_element_type | solution.py:27
  31.3 1.2 multiply_convert_fusion
  32.5 0.0 copy-done.2
  32.5 0.0 copy-done.4
  32.5 1.5 %fusion.14 = f32[16,4,256]{2,0,1:T(8,128)S(1)} fusion(bf16[16,4,2048]{2,0,1:T(8,128)(2,1)S(1)} %multiply_convert_fusion, bf16[2048,256]{1,0:T(8,128)(2,1)} %param.16, f32[256]{0:T(256)S(1)} %copy-done.4, f32[256]{0:T(256)S(1)} %copy-done.2), kind=kOutput, calls=%fused_computation.21 | convolution fusion | flops 67223552 | bytes 1378304 | tf_op jit(solution)/shard_map/dot_general | solution.py:33
  34.1 1.5 %fusion.7 = f32[16,4,256]{2,0,1:T(8,128)S(1)} fusion(bf16[16,4,2048]{2,0,1:T(8,128)(2,1)S(1)} %multiply_convert_fusion, bf16[2048,256]{1,0:T(8,128)(2,1)} %param.17), kind=kOutput, calls=%fused_computation.13 | convolution fusion | flops 67141632 | bytes 1376256 | tf_op jit(solution)/shard_map/dot_general | solution.py:34
  35.6 0.7 reshape.132
  36.3 2.2 %divide_multiply_fusion = f32[16,4,256]{2,0,1:T(8,128)} fusion(bf16[16,4,2048]{2,0,1:T(8,128)(2,1)S(1)} %multiply_convert_fusion, bf16[2048,256]{1,0:T(8,128)(2,1)} %param.15), kind=kOutput, calls=%fused_computation.53 | convolution fusion | flops 67207168 | bytes 1376256 | tf_op jit(solution)/shard_map/dot_general | solution.py:32
  38.4 0.9 reshape.121
  39.4 0.8 slice_bitcast_fusion.6
  40.1 2.8 %fusion.4 = f32[16,2,1,128]{3,2,1,0:T(1,128)S(1)} fusion(f32[16,2,128,1]{2,3,1,0:T(1,128)S(1)} %bitcast.149, f32[16,2,128,128]{3,2,1,0:T(8,128)S(1)} %add_select_fusion, f32[16,2,128]{2,1,0:T(2,128)S(1)} %get-tuple-element.24, f32[16,2,128]{2,1,0:T(2,128)S(1)} %get-tuple-element.20, f32[16,2,128]{2,1,0:T(2,128)S(1)} %get-tuple-element.47), kind=kOutput, calls=%fused_computation.8 | convolution fusion | flops 7864320 | bytes 2179072 | tf_op jit(solution)/shard_map/bhk,bhkv->bhv/dot_general | solution.py:62
  43.0 4.3 %fusion.35 = f32[16,2,1,128]{3,2,1,0:T(1,128)S(1)} fusion(f32[16,2,128,1]{2,3,1,0:T(1,128)S(1)} %bitcast.158, f32[16,2,128,128]{3,2,1,0:T(8,128)S(1)} %add_select_fusion, f32[16,2,128]{2,1,0:T(2,128)S(1)} %get-tuple-element.27, f32[16,2,128]{2,1,0:T(2,128)S(1)} %get-tuple-element.23, f32[16,2,128]{2,1,0:T(2,128)S(1)} %get-tuple-element.44, ...), kind=kOutput, calls=%fused_computation.45 | convolution fusion | flops 9437184 | bytes 2228224 | tf_op jit(solution)/shard_map/bhk,bhkv->bhv/dot_general | solution.py:62
  47.2 6.1 %fusion.5 = f32[16,2,1,128]{3,2,1,0:T(1,128)S(1)} fusion(f32[16,2,128,1]{2,3,1,0:T(1,128)S(1)} %bitcast.157, f32[16,2,128]{2,1,0:T(2,128)S(1)} %get-tuple-element.26, f32[16,2,128]{2,1,0:T(2,128)S(1)} %get-tuple-element.22, f32[16,2,128]{2,1,0:T(2,128)S(1)} %get-tuple-element.45, f32[16,2,128,128]{3,2,1,0:T(8,128)S(1)} %add_select_fusion, ...), kind=kOutput, calls=%fused_computation.9 | convolution fusion | flops 11010048 | bytes 2277376 | tf_op jit(solution)/shard_map/bhk,bhkv->bhv/dot_general | solution.py:62
  53.3 0.0 copy-start.6
  53.3 7.2 %fusion = f32[16,2,1,128]{3,2,1,0:T(1,128)S(1)} fusion(f32[16,2,128,1]{2,3,1,0:T(1,128)S(1)} %bitcast.156, f32[16,2,128]{2,1,0:T(2,128)S(1)} %get-tuple-element.25, f32[16,2,128]{2,1,0:T(2,128)S(1)} %get-tuple-element.21, f32[16,2,128]{2,1,0:T(2,128)S(1)} %get-tuple-element.46, f32[16,2,128]{2,1,0:T(2,128)S(1)} %get-tuple-element.26, ...), kind=kOutput, calls=%fused_computation | convolution fusion | flops 12582912 | bytes 2326528 | tf_op jit(solution)/shard_map/bhk,bhkv->bhv/dot_general | solution.py:62
  60.6 0.1 fusion.39
  60.8 0.1 mul.343
  60.9 0.1 mul.344
  61.0 0.0 copy-done
  61.0 2.8 %fusion.16 = f32[16,4,2048]{2,0,1:T(8,128)} fusion(bf16[1024,2048]{1,0:T(8,128)(2,1)} %param.19, s32[]{:T(128)S(6)} %select_n.20, f32[16,4,256]{2,0,1:T(8,128)S(1)} %mul.344, f32[16,1,256]{2,0,1:T(8,128)S(1)} %stack.28, f32[16,1,256]{2,0,1:T(8,128)S(1)} %stack.27, f32[16,1,256]{2,0,1:T(8,128)S(1)} %stack.26, f32[16,1,256]{2,0,1:T(8,128)S(1)} %stack.25, ...), kind=kOutput, calls=%fused_computation.24 | convolution fusion | flops 134430720 | bytes 3015684 | tf_op jit(solution)/shard_map/dot_general | solution.py:72
  63.8 0.0 all-gather.3.cloned.1.call-update
  63.9 24.1 %all-gather.3.cloned.1.call-done = f32[64,4,2048]{2,0,1:T(8,128)} async-done(((f32[16,4,2048]{2,0,1:T(8,128)}), f32[64,4,2048]{2,0,1:T(8,128)}) %all-gather.3.cloned.1.call-update) | async-done | bytes 2097168 | tf_op jit(solution)/shard_map/all_gather | solution.py:75
  88.0 1.8 %reduce_sum.38 = bf16[16,4,2048]{2,0,1:T(8,128)(2,1)S(1)} reduce(f32[4,16,4,2048]{3,1,0,2:T(8,128)} %bitcast.143, f32[]{:T(128)} %constant.13.clone.1), dimensions={0}, to_apply=%region_3.4 | reduce | flops 393216 | bytes 2359300 | tf_op jit(solution)/shard_map/reduce_sum | solution.py:75
  89.8 1.4 %copy.71 = bf16[16,4,2048]{0,1,2:T(4,128)(2,1)S(1)} copy(bf16[16,4,2048]{2,0,1:T(8,128)(2,1)S(1)} %reduce_sum.38) | data formatting | bytes 524288 | tf_op jit(solution)/shard_map/convert_element_type | solution.py:78
  91.1 2.2 %reshape.149 = bf16[8,2,8192]{2,1,0:T(2,128)(2,1)S(1)} reshape(bf16[2048,4,16]{2,1,0:T(4,128)(2,1)S(1)} %bitcast.141) | data formatting | bytes 524288
  93.3 14.7 %all_to_all.27 = bf16[8,2,8192]{2,1,0:T(2,128)(2,1)} all-to-all(bf16[8,2,8192]{2,1,0:T(2,128)(2,1)S(1)} %reshape.149), channel_id=1, replica_groups=mesh['kv'=8,'tp'=4] {'kv'}, dimensions={0} | all-to-all | bytes 524288 | tf_op jit(solution)/shard_map/all_to_all | solution.py:79
  108.0 2.4 %reshape.150 = bf16[2048,4,16]{2,1,0:T(4,128)(2,1)S(1)} reshape(bf16[8,2,8192]{2,1,0:T(2,128)(2,1)} %all_to_all.27) | data formatting | bytes 524288
  110.4 1.1 copy.84
  111.6 0.9 copy.74
  (18 shorter events, 0.3 us)
Async XLA Ops:
  7.2 53.8 %copy-start = (bf16[2048,256]{1,0:T(8,128)(2,1)S(1)}, bf16[2048,256]{1,0:T(8,128)(2,1)}, u32[]{:S(2)}) copy-start(bf16[2048,256]{1,0:T(8,128)(2,1)} %param.18) | copy-start | bytes 3145732
  7.2 20.7 %all-to-all-start = ((bf16[128,4,256]{2,1,0:T(4,128)(2,1)}), bf16[128,4,256]{2,1,0:T(4,128)(2,1)S(1)}, u32[]{:S(2)}, u32[]{:S(2)}) async-start(bf16[128,4,256]{2,1,0:T(4,128)(2,1)} %param.13), calls=%async_computation | async-start | bytes 524288 | tf_op jit(solution)/shard_map/all_to_all | solution.py:26
  14.6 73.4 %all-gather.3.cloned.1.call-start = ((), (), s32[]{:S(2)}) async-start(), calls=%async_computation.2 | async-start | bytes 2621440 | tf_op jit(solution)/shard_map/all_gather | solution.py:75
  15.3 0.6 copy-start.3
  27.8 25.5 %copy-start.1 = (f32[16,2,128,128]{3,2,1,0:T(8,128)}, f32[16,2,128,128]{3,2,1,0:T(8,128)S(1)}, u32[]{:S(2)}) copy-start(f32[16,2,128,128]{3,2,1,0:T(8,128)S(1)} %add_select_fusion) | copy-start | bytes 6291460
  27.8 3.5 %copy-start.5 = (f32[2048]{0:T(1024)S(1)}, f32[2048]{0:T(1024)}, u32[]{:S(2)}) copy-start(f32[2048]{0:T(1024)} %param.14) | copy-start | bytes 24580
  27.9 4.6 %copy-start.2 = (f32[256]{0:T(256)S(1)}, f32[256]{0:T(256)}, u32[]{:S(2)}) copy-start(f32[256]{0:T(256)} %param.20) | copy-start | bytes 3076
  27.9 4.6 %copy-start.4 = (f32[256]{0:T(256)S(1)}, f32[256]{0:T(256)}, u32[]{:S(2)}) copy-start(f32[256]{0:T(256)} %copy-done.3) | copy-start | bytes 3076
  53.3 7.7 %copy-start.6 = (f32[256]{0:T(256)S(1)}, f32[256]{0:T(256)}, u32[]{:S(2)}) copy-start(f32[256]{0:T(256)} %broadcast_bitcast_fusion) | copy-start | bytes 3076
Sparse Core Ops, SparseCore 0:
  64.0 23.9 all-gather.2
